TPU v7x, 32 devices: a whole 2x2x4 slice. The times are simulated.
32 devices in a mesh: ep: 8 (over z, x), tp: 4 (over y, core).
Axes of the slice: x: 2, y: 2, z: 4, core: 2. Of those that a mesh axis runs over, the one named last changes fastest.
Arguments:
- conv_gate: bfloat16 [4096, 2048], P('ep', 'tp'), may hold values from -6 to 6
- conv_in_gate: bfloat16 [4096, 2048], P('ep', 'tp'), may hold values from -6 to 6
- conv_value: bfloat16 [4096, 2048], P('ep', 'tp'), may hold values from -6 to 6
- conv_taps: float32 [3, 2048], P(None, 'tp'), may hold values from -3.5 to 3.5
- mix_out_weight: bfloat16 [2048, 4096], P(None, 'tp'), may hold values from -0.125 to 0.125
- expert_input: bfloat16 [1280, 4096], P('ep', 'tp'), may hold values from -1600 to 1600
- expert_gain: float32 [4096], replicated, may hold values from 0.1 to 1.9
- routes: int32 [1280, 2], P('ep'), may hold values from 0 to 7, all different within a row; in each aligned block of 160 rows (0 to 159, 160 to 319, ...) at most 60 rows name the same one
- group_prob: float32 [1280], P('ep'), may hold values from 0.3 to 1
- pair_logits: float32 [1280, 2], P('ep'), may hold values from -6 to 6
- expert_gate: bfloat16 [8, 4096, 2048], P('ep', None, 'tp'), may hold values from -0.09375 to 0.09375
- expert_up: bfloat16 [8, 4096, 2048], P('ep', None, 'tp'), may hold values from -0.09375 to 0.09375
- expert_down: bfloat16 [8, 2048, 4096], P('ep', None, 'tp'), may hold values from -0.125 to 0.125
Outputs:
- mixed: bfloat16 [4096, 4096], P('ep', 'tp')
- expert_output: bfloat16 [1280, 4096], P('ep', 'tp')
Inputs may be any that keep to these rules, and one draw needn't show every extreme that they name: `routes`: in the 160 rows of one index of ep no expert is named by more than 60 rows, a bound that some block reaches; each row names 2 different experts.
All inputs are finite; a program needn't handle non-finite values.
Results may differ from a plain program's by a relative error of at most 0.0071.
Values may be sent and summed in bfloat16 or wider, within the bound.
A program may use at most 64 MiB of HBM per device.

v0:
```python
import jax
import jax.numpy as jnp
from jax import lax
from jax.sharding import PartitionSpec as P

D = 4096


EPS = 1e-06


def shifted(block, axis, distance):
    devices = range(lax.axis_size(axis))
    route = [(i - distance, i) for i in devices if i - distance in devices]
    return lax.ppermute(block, axis, route)


def slot_table(route_block, capacity, expert_count):
    pair_ids = route_block.reshape(-1)
    onehot = (pair_ids[:, None] == jnp.arange(expert_count, dtype=jnp.int32)[None, :]).astype(
        jnp.int32
    )
    earlier = jnp.cumsum(onehot, axis=0) - onehot
    within = jnp.sum(earlier * onehot, axis=1)
    return pair_ids * capacity + within


def pair_weights(group_prob, pair_logits):
    spread = pair_logits[:, 0] - pair_logits[:, 1]
    return (
        jnp.stack([jax.nn.sigmoid(spread), jax.nn.sigmoid(-spread)], axis=1) * group_prob[:, None]
    )


def per_device(
    conv_gate,
    conv_in_gate,
    conv_value,
    conv_taps,
    mix_out_weight,
    expert_input,
    expert_gain,
    routes,
    group_prob,
    pair_logits,
    expert_gate,
    expert_up,
    expert_down,
):
    reach = conv_taps.shape[0] - 1
    token_rows = conv_value.shape[0]
    products = conv_in_gate.astype(jnp.float32) * conv_value.astype(jnp.float32)
    earlier_rows = shifted(products[token_rows - reach :], "ep", 1)
    padded = jnp.concatenate([earlier_rows, products], axis=0)
    convolved = jnp.zeros_like(products)
    for offset in range(reach + 1):
        convolved = convolved + conv_taps[offset][None, :] * padded[offset : offset + token_rows]
    mixer_rows = (conv_gate.astype(jnp.float32) * convolved).astype(jnp.bfloat16)
    mixed = jnp.dot(
        lax.all_gather(mixer_rows, "tp", axis=1, tiled=True),
        mix_out_weight,
        preferred_element_type=jnp.float32,
    ).astype(jnp.bfloat16)
    expert_count = lax.axis_size("ep")
    tok_rows, choose_count = routes.shape
    capacity = 3 * tok_rows * choose_count // (2 * expert_count)
    slot_index = slot_table(routes, capacity, expert_count)
    pair_row = jnp.arange(tok_rows * choose_count, dtype=jnp.int32) // choose_count
    slot_rows = expert_count * capacity
    gate_block = expert_gate[0]
    up_block = expert_up[0]
    down_block = expert_down[0]
    columns = expert_input.shape[1]
    features = expert_input.astype(jnp.float32)
    squares = lax.psum(jnp.sum(features * features, axis=1), "tp")
    scale = lax.rsqrt(squares / D + EPS)
    gain_part = lax.dynamic_slice_in_dim(expert_gain, lax.axis_index("tp") * columns, columns, 0)
    normed = (features * scale[:, None] * gain_part[None, :]).astype(jnp.bfloat16)
    buffer = jnp.zeros((slot_rows, columns), jnp.bfloat16).at[slot_index].set(normed[pair_row])
    arrived = lax.all_to_all(
        buffer.reshape(expert_count, capacity, columns),
        "ep",
        split_axis=0,
        concat_axis=0,
        tiled=True,
    ).reshape(slot_rows, columns)
    shard_piece = lax.all_gather(arrived, "tp", axis=1, tiled=True)
    gate_sum = jnp.dot(shard_piece, gate_block, preferred_element_type=jnp.float32)
    up_sum = jnp.dot(shard_piece, up_block, preferred_element_type=jnp.float32)
    hidden = (jax.nn.silu(gate_sum) * up_sum).astype(jnp.bfloat16)
    results = jnp.dot(
        lax.all_gather(hidden, "tp", axis=1, tiled=True),
        down_block,
        preferred_element_type=jnp.float32,
    ).astype(jnp.bfloat16)
    returned = lax.all_to_all(
        results.reshape(expert_count, capacity, down_block.shape[1]),
        "ep",
        split_axis=0,
        concat_axis=0,
        tiled=True,
    ).reshape(slot_rows, down_block.shape[1])
    picked = (
        returned[slot_index]
        .reshape(tok_rows, choose_count, down_block.shape[1])
        .astype(jnp.float32)
    )
    weights = pair_weights(group_prob, pair_logits)
    expert_output = jnp.sum(picked * weights[:, :, None], axis=1).astype(jnp.bfloat16)
    return (mixed, expert_output)


def solution(mesh):
    in_specs = (
        P("ep", "tp"),
        P("ep", "tp"),
        P("ep", "tp"),
        P(None, "tp"),
        P(None, "tp"),
        P("ep", "tp"),
        P(),
        P("ep", None),
        P("ep"),
        P("ep", None),
        P("ep", None, "tp"),
        P("ep", None, "tp"),
        P("ep", None, "tp"),
    )
    out_specs = (P("ep", "tp"), P("ep", "tp"))
    return jax.shard_map(
        per_device, mesh=mesh, in_specs=in_specs, out_specs=out_specs, check_vma=False
    )
```

profile of v0, /device:TPU:1, one launch (start us, length us, event | category | flops | bytes accessed | tf_op | source)
XLA Modules:
  0.0 169.3 jit_solution(3366997663291530493)
XLA Ops:
  7.2 0.0 all-gather.6.cloned.1.call-start
  7.2 0.8 copy.17
  8.0 0.7 broadcast_multiply_fusion
  8.7 0.1 eq.22
  8.9 0.9 reduce-window.6
  9.8 0.2 slice_reduce_fusion
  10.0 0.1 add_bitcast_fusion
  10.1 0.1 copy.16
  10.2 0.1 mul.117
  10.4 1.1 fusion.22
  11.5 6.4 %psum.7 = f32[160]{0:T(256)S(1)} all-reduce(f32[160]{0:T(256)S(1)} %fusion.22), channel_id=1, replica_groups=mesh['ep'=8,'tp'=4] {'tp'}, use_global_device_ids=true, to_apply=%region_4.5 | all-reduce | flops 160 | bytes 1280 | tf_op jit(solution)/shard_map/psum | solution.py:75
  17.9 0.7 dynamic_slice.3
  18.6 1.1 fusion.24
  19.8 4.5 %scatter_custom_fusion = bf16[480,1024]{1,0:T(8,128)(2,1)S(1)} fusion(s32[320]{0:T(512)S(1)} %fusion.30, bf16[160,1024]{1,0:T(8,128)(2,1)S(1)} %fusion.24, s32[1024]{0:T(1024)S(1)} %pad_clamp_fusion.1, bf16[]{:T(256)} %constant.18.clone.1), kind=kCustom, calls=%fused_computation.30 | custom fusion | bytes 983042 | tf_op jit(solution)/shard_map/scatter | solution.py:79
  24.3 0.2 reshape.137
  24.4 30.2 %all_to_all.10 = bf16[8,60,1024]{2,1,0:T(8,128)(2,1)S(1)} all-to-all(bf16[8,60,1024]{2,1,0:T(8,128)(2,1)S(1)} %reshape.137), channel_id=1, replica_groups=mesh['ep'=8,'tp'=4] {'ep'}, dimensions={0} | all-to-all | bytes 1966080 | tf_op jit(solution)/shard_map/all_to_all | solution.py:80
  54.6 1.1 reshape.138
  55.8 0.0 all-gather.6.cloned.1.call-update
  55.8 0.0 all-gather.8.cloned.1.call-start
  55.8 33.8 %all-gather.6.cloned.1.call-done = bf16[480,4096]{1,0:T(8,128)(2,1)} async-done(((bf16[480,1024]{1,0:T(8,128)(2,1)}), bf16[480,4096]{1,0:T(8,128)(2,1)}) %all-gather.6.cloned.1.call-update) | async-done | bytes 3932176 | tf_op jit(solution)/shard_map/all_gather | solution.py:87
  89.7 5.7 %fusion.4 = f32[480,512]{1,0:T(8,128)S(1)} fusion(bf16[480,4096]{1,0:T(8,128)(2,1)} %all-gather.6.cloned.1.call-done, bf16[1,4096,512]{2,1,0:T(8,128)(2,1)} %param.23), kind=kOutput, calls=%fused_computation.7 | convolution fusion | flops 2013265920 | bytes 9109504 | tf_op jit(solution)/shard_map/dot_general | solution.py:88
  95.4 0.0 copy-done.6
  95.4 0.0 copy-done.7
  95.4 3.0 %fusion.12 = bf16[480,512]{1,0:T(8,128)(2,1)} fusion(bf16[480,4096]{1,0:T(8,128)(2,1)S(1)} %copy-done.7, bf16[1,4096,512]{2,1,0:T(8,128)(2,1)S(1)} %copy-done.6, f32[480,512]{1,0:T(8,128)S(1)} %fusion.4), kind=kOutput, calls=%fused_computation.13 | convolution fusion | flops 2014740480 | bytes 9601024 | tf_op jit(solution)/shard_map/dot_general | solution.py:89
  98.5 0.0 all-gather.8.cloned.1.call-update
  98.5 0.0 all-gather.4.cloned.1.call-start
  98.6 0.0 copy-done.1
  98.6 0.0 copy-done.2
  98.6 0.1 convert_multiply_fusion
  98.8 3.1 %collective-permute-start = (f32[2,512]{1,0:T(2,128)S(1)}, f32[2,512]{1,0:T(2,128)S(1)}, u32[]{:S(2)}, u32[]{:S(2)}) collective-permute-start(f32[2,512]{1,0:T(2,128)S(1)} %slice.48), channel_id=1, source_target_pairs={{0,4},{4,8},{8,12},{12,16},{16,20},{20,24},{24,28},{1,5},{5,9},{9,... | collective-permute-start | bytes 12296 | tf_op jit(solution)/shard_map/ppermute | solution.py:15
  101.9 0.0 copy-done.3
  101.9 0.7 collective-permute-done
  102.6 1.2 fusion.20
  103.8 0.0 all-gather.4.cloned.1.call-update
  103.8 16.7 %all-gather.8.cloned.1.call-done = bf16[480,2048]{1,0:T(8,128)(2,1)} async-done(((bf16[480,512]{1,0:T(8,128)(2,1)}), bf16[480,2048]{1,0:T(8,128)(2,1)}) %all-gather.8.cloned.1.call-update) | async-done | bytes 1966096 | tf_op jit(solution)/shard_map/all_gather | solution.py:92
  120.5 5.0 %fusion.6 = bf16[480,1024]{1,0:T(8,128)(2,1)S(1)} fusion(bf16[480,2048]{1,0:T(8,128)(2,1)} %all-gather.8.cloned.1.call-done, bf16[1,2048,1024]{2,1,0:T(8,128)(2,1)} %param.25), kind=kOutput, calls=%fused_computation.10 | convolution fusion | flops 2013757440 | bytes 7143424 | tf_op jit(solution)/shard_map/dot_general | solution.py:91
  125.5 0.0 copy-start.4
  125.5 0.0 copy-start.5
  125.5 1.2 reshape.139
  126.7 5.2 %all-to-all-start.1 = ((bf16[8,60,1024]{2,1,0:T(8,128)(2,1)}), bf16[8,60,1024]{2,1,0:T(8,128)(2,1)S(1)}, u32[]{:S(2)}, u32[]{:S(2)}) async-start(bf16[8,60,1024]{2,1,0:T(8,128)(2,1)} %reshape.139), calls=%async_computation.1 | async-start | bytes 2097152 | tf_op jit(solution)/shard_map/all_to_all | solution.py:96
  132.0 0.1 copy.18
  132.1 13.1 %all-gather.4.cloned.1.call-done = bf16[512,2048]{1,0:T(8,128)(2,1)} async-done(((bf16[512,512]{1,0:T(8,128)(2,1)}), bf16[512,2048]{1,0:T(8,128)(2,1)}) %all-gather.4.cloned.1.call-update) | async-done | bytes 2097168 | tf_op jit(solution)/shard_map/all_gather | solution.py:60
  145.2 6.1 %convolution_convert_fusion = bf16[512,1024]{1,0:T(8,128)(2,1)} fusion(bf16[512,2048]{1,0:T(8,128)(2,1)} %all-gather.4.cloned.1.call-done, bf16[2048,1024]{1,0:T(8,128)(2,1)} %param.17), kind=kOutput, calls=%fused_computation.9 | convolution fusion | flops 2148007936 | bytes 7340032 | tf_op jit(solution)/shard_map/dot_general | solution.py:59
  151.4 5.9 %all-to-all-done.1 = bf16[8,60,1024]{2,1,0:T(8,128)(2,1)S(1)} async-done(((bf16[8,60,1024]{2,1,0:T(8,128)(2,1)}), bf16[8,60,1024]{2,1,0:T(8,128)(2,1)S(1)}, u32[]{:S(2)}, u32[]{:S(2)}) %all-to-all-start.1) | async-done | bytes 983072 | tf_op jit(solution)/shard_map/all_to_all | solution.py:96
  157.2 0.2 reshape.140
  157.4 2.1 %gather_fusion = bf16[320,1024]{1,0:T(8,128)(2,1)S(1)} fusion(bf16[480,1024]{1,0:T(8,128)(2,1)S(1)} %reshape.140, s32[1024]{0:T(1024)S(1)} %pad_clamp_fusion), kind=kCustom, calls=%fused_computation.1 | custom fusion | bytes 1312000 | tf_op jit(solution)/shard_map/gather | solution.py:104
  159.5 0.8 reshape.142
  160.3 2.4 %multiply_reduce_fusion = bf16[160,1024]{1,0:T(8,128)(2,1)} fusion(f32[160,2,1024]{2,1,0:T(2,128)S(1)} %reshape.142, f32[160,2]{1,0:T(8,128)S(1)} %copy.18), kind=kLoop, calls=%fused_computation.12 | loop fusion | flops 491520 | bytes 1639680 | tf_op jit(solution)/shard_map/reduce_sum | solution.py:109
  (23 shorter events, 0.2 us)
Async XLA Ops:
  7.2 82.5 %all-gather.6.cloned.1.call-start = ((), (), s32[]{:S(2)}) async-start(), calls=%async_computation.3 | async-start | bytes 4915200 | tf_op jit(solution)/shard_map/all_gather | solution.py:87
  55.8 64.7 %all-gather.8.cloned.1.call-start = ((), (), s32[]{:S(2)}) async-start(), calls=%async_computation.4 | async-start | bytes 2457600 | tf_op jit(solution)/shard_map/all_gather | solution.py:92
  89.7 5.7 %copy-start.6 = (bf16[1,4096,512]{2,1,0:T(8,128)(2,1)S(1)}, bf16[1,4096,512]{2,1,0:T(8,128)(2,1)}, u32[]{:S(2)}) copy-start(bf16[1,4096,512]{2,1,0:T(8,128)(2,1)} %param.24) | copy-start | bytes 12582916
  89.7 5.8 %copy-start.7 = (bf16[480,4096]{1,0:T(8,128)(2,1)S(1)}, bf16[480,4096]{1,0:T(8,128)(2,1)}, u32[]{:S(2)}) copy-start(bf16[480,4096]{1,0:T(8,128)(2,1)} %all-gather.6.cloned.1.call-done) | copy-start | bytes 11796484
  95.4 3.1 %copy-start.1 = (bf16[512,512]{1,0:T(8,128)(2,1)S(1)}, bf16[512,512]{1,0:T(8,128)(2,1)}, u32[]{:S(2)}) copy-start(bf16[512,512]{1,0:T(8,128)(2,1)} %param.15) | copy-start | bytes 1572868
  95.4 3.1 %copy-start.2 = (bf16[512,512]{1,0:T(8,128)(2,1)S(1)}, bf16[512,512]{1,0:T(8,128)(2,1)}, u32[]{:S(2)}) copy-start(bf16[512,512]{1,0:T(8,128)(2,1)} %param.14) | copy-start | bytes 1572868
  95.4 6.4 %copy-start.3 = (f32[3,512]{1,0:T(4,128)S(1)}, f32[3,512]{1,0:T(4,128)}, u32[]{:S(2)}) copy-start(f32[3,512]{1,0:T(4,128)} %param.16) | copy-start | bytes 18436
  95.4 7.2 %copy-start = (bf16[512,512]{1,0:T(8,128)(2,1)S(1)}, bf16[512,512]{1,0:T(8,128)(2,1)}, u32[]{:S(2)}) copy-start(bf16[512,512]{1,0:T(8,128)(2,1)} %param.13) | copy-start | bytes 1572868
  98.5 46.7 %all-gather.4.cloned.1.call-start = ((), (), s32[]{:S(2)}) async-start(), calls=%async_computation.2 | async-start | bytes 2621440 | tf_op jit(solution)/shard_map/all_gather | solution.py:60
  98.8 3.8 %collective-permute-start = (f32[2,512]{1,0:T(2,128)S(1)}, f32[2,512]{1,0:T(2,128)S(1)}, u32[]{:S(2)}, u32[]{:S(2)}) collective-permute-start(f32[2,512]{1,0:T(2,128)S(1)} %slice.48), channel_id=1, source_target_pairs={{0,4},{4,8},{8,12},{12,16},{16,20},{20,24},{24,28},{1,5},{5,9},{9,... | collective-permute-start | bytes 12296 | tf_op jit(solution)/shard_map/ppermute | solution.py:15
  125.5 6.4 %copy-start.4 = (f32[160,2]{0,1:T(2,128)S(1)}, f32[160,2]{0,1:T(2,128)}, u32[]{:S(2)}) copy-start(f32[160,2]{0,1:T(2,128)} %param.22) | copy-start | bytes 3844
  125.5 6.4 %copy-start.5 = (f32[160]{0:T(256)S(1)}, f32[160]{0:T(256)}, u32[]{:S(2)}) copy-start(f32[160]{0:T(256)} %param.21) | copy-start | bytes 1924
  126.7 30.6 %all-to-all-start.1 = ((bf16[8,60,1024]{2,1,0:T(8,128)(2,1)}), bf16[8,60,1024]{2,1,0:T(8,128)(2,1)S(1)}, u32[]{:S(2)}, u32[]{:S(2)}) async-start(bf16[8,60,1024]{2,1,0:T(8,128)(2,1)} %reshape.139), calls=%async_computation.1 | async-start | bytes 2097152 | tf_op jit(solution)/shard_map/all_to_all | solution.py:96
Sparse Core Ops, SparseCore 0:
  55.9 33.7 all-gather.5
  98.6 21.8 all-gather.7
  122.6 22.5 all-gather.3
where the time goes:
time: 171 us; the launch traced here: 169 us
  waiting for transfers between devices  70.3 us (41%)
  blocking collectives  36.6 us (21%)
  matrix products  19.9 us (12%)
  between operations  14 us (8%)
  local copies, waits for them, and re-layouts  12.3 us (7%)
  starting transfers between devices  8.44 us (5%)
  other arithmetic  7.81 us (5%)
    all_gather x1, waiting for transfers between devices, per_device(): shard_piece = lax.all_gather(arrived, 'tp', axis=1, tiled=True)  33.8 us
    all_to_all x1, blocking collectives, per_device(): lax.all_to_all(buffer.reshape(expert_count, capacity, columns), 'ep', spl...  30.2 us
    all_gather x1, waiting for transfers between devices, per_device(): lax.all_gather(hidden, 'tp', axis=1, tiled=True)  16.7 us
    all_gather x1, waiting for transfers between devices, per_device(): lax.all_gather(mixer_rows, 'tp', axis=1, tiled=True)  13.1 us
    psum x1, blocking collectives, per_device(): squares = lax.psum(jnp.sum(features * features, axis=1), 'tp')  6.4 us
    dot_general x1, matrix products, per_device(): jnp.dot(lax.all_gather(mixer_rows, 'tp', axis=1, tiled=True), mix_out_wei...  6.12 us
    all_to_all x1, waiting for transfers between devices, per_device(): lax.all_to_all(results.reshape(expert_count, capacity, down_block.shape[1...  5.89 us
    dot_general x1, matrix products, per_device(): jnp.dot(shard_piece, gate_block, preferred_element_type=jnp.float32)  5.71 us
  transfers between devices with their start and end apart: 5, of which 5 were waited for; matrix products, arithmetic and copies ran while one was open for 8% of the time, Pallas kernels for 0%

commit v1 on v0

--- a/solution.py
+++ b/solution.py
@@ -1,6 +1,10 @@
+import functools
+
 import jax
 import jax.numpy as jnp
 from jax import lax
+from jax.experimental import pallas as pl
+from jax.experimental.pallas import tpu as pltpu
 from jax.sharding import PartitionSpec as P
 
 D = 4096
@@ -110,7 +114,440 @@
     return (mixed, expert_output)
 
 
+CHUNKS = 2
+CORES = 2
+HALVES = 2
+MESH = pl.DeviceIdType.MESH
+
+
+def fused_kernel(
+    n,
+    cap,
+    pitch,
+    gate_h,
+    ingate_h,
+    value_h,
+    taps_ref,
+    wmix_h,
+    x_ref,
+    gain_ref,
+    routes_ref,
+    prob_ref,
+    logits_ref,
+    lanes_ref,
+    wg_h,
+    wu_h,
+    wd_h,
+    mixed_ref,
+    out_ref,
+    gate_v,
+    ingate_v,
+    value_v,
+    wmix_v,
+    wg_v,
+    wu_v,
+    wd_v,
+    halo,
+    padded,
+    rows_all,
+    picks,
+    outgoing,
+    arrived,
+    normed,
+    hidden,
+    results,
+    returned,
+    total,
+    local_sem,
+    halo_send,
+    halo_recv,
+    xz_send,
+    xz_recv,
+    xt_send,
+    xt_recv,
+    h_send,
+    h_recv,
+    m_send,
+    m_recv,
+    ret_send,
+    ret_recv,
+):
+    e = lax.axis_index("ep")
+    t = lax.axis_index("tp")
+    core = lax.rem(t, CORES)
+    t_core = t + 1 - 2 * core
+    t_far = lax.rem(t + CORES, 2 * CORES)
+    t_far_core = lax.rem(t_core + CORES, 2 * CORES)
+    tok_b, columns = x_ref.shape
+    tok_a, channels = gate_v.shape
+    tp = arrived.shape[0]
+    width = columns * tp
+    ff = wg_v.shape[1]
+    chunk_rows = n * pitch // CHUNKS
+    per_chunk = n // CHUNKS
+    half_rows = tok_a // HALVES
+    tail = halo.shape[1]
+
+    loads = [
+        pltpu.make_async_copy(ingate_h, ingate_v, local_sem.at[0]),
+        pltpu.make_async_copy(value_h, value_v, local_sem.at[1]),
+        pltpu.make_async_copy(gate_h, gate_v, local_sem.at[2]),
+        pltpu.make_async_copy(wg_h.at[0], wg_v, local_sem.at[3]),
+        pltpu.make_async_copy(wu_h.at[0], wu_v, local_sem.at[4]),
+        pltpu.make_async_copy(wd_h.at[0], wd_v, local_sem.at[5]),
+        pltpu.make_async_copy(wmix_h, wmix_v, local_sem.at[6]),
+    ]
+    for load in loads:
+        load.start()
+
+    low = cap // 16 * 16
+    if cap < pitch:
+        for k in range(n):
+            spare = pl.ds(k * pitch + low, pitch - low)
+            for s in range(tp):
+                arrived[s, spare, :] = jnp.zeros((pitch - low, columns), jnp.bfloat16)
+            returned[spare, :] = jnp.zeros((pitch - low, columns), jnp.bfloat16)
+
+    barrier = pltpu.get_barrier_semaphore()
+    for k in range(1, n):
+        pl.semaphore_signal(barrier, inc=1, device_id=(e ^ k, t), device_id_type=MESH)
+    pl.semaphore_signal(barrier, inc=1, device_id=(e, t_core), device_id_type=MESH)
+    pl.semaphore_signal(barrier, inc=1, device_id=(e, t_far), device_id_type=MESH)
+
+    def block(k):
+        return pl.ds(k * pitch, cap)
+
+    expert_of = lanes_ref[0:1, :] ^ e
+    place_of = lanes_ref[1:2, :]
+    first = (routes_ref[:, 0:1] == expert_of).astype(jnp.float32)
+    second = (routes_ref[:, 1:2] == expert_of).astype(jnp.float32)
+    named = first + second
+    earlier = (
+        lax.broadcasted_iota(jnp.int32, (tok_b, tok_b), 1)
+        < lax.broadcasted_iota(jnp.int32, (tok_b, tok_b), 0)
+    ).astype(jnp.float32)
+    within = jnp.dot(
+        earlier.astype(jnp.bfloat16),
+        named.astype(jnp.bfloat16),
+        preferred_element_type=jnp.float32,
+    )
+    here = (within == place_of.astype(jnp.float32)).astype(jnp.float32)
+    spread = logits_ref[:, 0:1] - logits_ref[:, 1:2]
+    prob = prob_ref[...]
+    w_first = prob * jax.nn.sigmoid(spread)
+    w_second = prob * jax.nn.sigmoid(-spread)
+    pick = named * here
+    weighted = (first * w_first + second * w_second) * here
+    high = weighted.astype(jnp.bfloat16)
+    picks[0] = high
+    picks[1] = (weighted - high.astype(jnp.float32)).astype(jnp.bfloat16)
+    outgoing[...] = lax.dot_general(
+        pick.astype(jnp.bfloat16),
+        x_ref[...],
+        (((0,), (0,)), ((), ())),
+        preferred_element_type=jnp.float32,
+    ).astype(jnp.bfloat16)
+    arrived[t, 0:pitch, :] = outgoing[0:pitch, :]
+
+    pl.semaphore_wait(barrier, n + 1)
+
+    xz = [None]
+    for k in range(1, n):
+        xz.append(
+            pltpu.make_async_remote_copy(
+                src_ref=outgoing.at[block(k)],
+                dst_ref=arrived.at[t, block(k)],
+                send_sem=xz_send.at[k],
+                recv_sem=xz_recv.at[k],
+                device_id=(e ^ k, t),
+                device_id_type=MESH,
+            )
+        )
+    for k in reversed(range(1, n)):
+        xz[k].start()
+
+    sent = []
+
+    def spread_to(ref, sel, sends, recvs, at):
+        def copy(s, way, target):
+            return pltpu.make_async_remote_copy(
+                src_ref=ref.at[s, sel],
+                dst_ref=ref.at[s, sel],
+                send_sem=sends.at[way, at],
+                recv_sem=recvs.at[way, at],
+                device_id=(e, target),
+                device_id_type=MESH,
+            )
+
+        far, near = copy(t, 0, t_far), copy(t, 1, t_core)
+        far.start()
+        near.start()
+        sent.append(far)
+        sent.append(near)
+
+        def relay():
+            copy(t_far, 0, t_far).wait_recv()
+            passed = copy(t_far, 2, t_core)
+            passed.start()
+            sent.append(passed)
+
+        def finish():
+            copy(t_core, 1, t_core).wait_recv()
+            copy(t_far_core, 2, t_core).wait_recv()
+
+        return relay, finish
+
+    loads[0].wait()
+    loads[1].wait()
+    next_e = lax.rem(e + 1, n)
+    tails = [
+        pltpu.make_async_remote_copy(
+            src_ref=source.at[pl.ds(tok_a - tail, tail)],
+            dst_ref=halo.at[i],
+            send_sem=halo_send.at[i],
+            recv_sem=halo_recv.at[i],
+            device_id=(next_e, t),
+            device_id_type=MESH,
+        )
+        for i, source in enumerate((ingate_v, value_v))
+    ]
+    for copy in tails:
+        copy.start()
+    top = 8
+    padded[top:, :] = ingate_v[...].astype(jnp.float32) * value_v[...].astype(jnp.float32)
+    for copy in tails:
+        copy.wait()
+    before = halo[0].astype(jnp.float32) * halo[1].astype(jnp.float32)
+    before = jnp.where(e > 0, before, jnp.zeros_like(before))
+    padded[0:top, :] = before[tail - top :, :]
+    loads[2].wait()
+    reach = taps_ref.shape[0] - 1
+    for half in range(HALVES):
+        base = half * half_rows
+        convolved = jnp.zeros((half_rows, channels), jnp.float32)
+        for offset in range(reach + 1):
+            convolved = (
+                convolved
+                + taps_ref[offset : offset + 1, :]
+                * padded[pl.ds(base + top - reach + offset, half_rows), :]
+            )
+        rows_all[t, pl.ds(base, half_rows), :] = (
+            gate_v[pl.ds(base, half_rows), :].astype(jnp.float32) * convolved
+        ).astype(jnp.bfloat16)
+    mix = []
+    mix.append(spread_to(rows_all, pl.ds(0, half_rows), m_send, m_recv, 0))
+
+    def chunk_of(j):
+        return (CHUNKS - 1 - j) * per_chunk
+
+    def forward(j):
+        stages = []
+        for k in reversed(range(chunk_of(j), chunk_of(j) + per_chunk)):
+            if k > 0:
+                xz[k].wait_recv()
+            stages.append(spread_to(arrived, block(k), xt_send, xt_recv, k))
+        return stages
+
+    def complete(stages):
+        for relay, _ in stages:
+            relay()
+        for _, finish in stages:
+            finish()
+
+    def mixer(half):
+        complete([mix[half]])
+        rows = pl.ds(half * half_rows, half_rows)
+        part = jnp.dot(
+            rows_all[0, rows, :], wmix_v[0:channels, :], preferred_element_type=jnp.float32
+        )
+        for s in range(1, tp):
+            part = part + jnp.dot(
+                rows_all[s, rows, :],
+                wmix_v[s * channels : (s + 1) * channels, :],
+                preferred_element_type=jnp.float32,
+            )
+        mixed_ref[rows, :] = part.astype(jnp.bfloat16)
+
+    back = {}
+    stages = forward(0)
+    for j in range(CHUNKS):
+        rows = pl.ds(chunk_of(j) * pitch, chunk_rows)
+        complete(stages)
+        squares = jnp.zeros((chunk_rows, 1), jnp.float32)
+        for s in range(tp):
+            block_f = arrived[s, rows, :].astype(jnp.float32)
+            squares = squares + jnp.sum(block_f * block_f, axis=1, keepdims=True)
+        scale = lax.rsqrt(squares / width + EPS)
+        for s in range(tp):
+            cols = slice(s * columns, (s + 1) * columns)
+            normed[:, cols] = (
+                arrived[s, rows, :].astype(jnp.float32) * scale * gain_ref[:, cols]
+            ).astype(jnp.bfloat16)
+        if j == 0:
+            loads[3].wait()
+            loads[4].wait()
+        gate_sum = jnp.dot(normed[...], wg_v[...], preferred_element_type=jnp.float32)
+        up_sum = jnp.dot(normed[...], wu_v[...], preferred_element_type=jnp.float32)
+        hidden[t, rows, :] = (gate_sum / (1.0 + jnp.exp(-gate_sum)) * up_sum).astype(jnp.bfloat16)
+        h_stage = spread_to(hidden, rows, h_send, h_recv, j)
+        if j == 0:
+            loads[6].wait()
+            mixer(0)
+        if j + 1 < CHUNKS:
+            stages = forward(j + 1)
+        else:
+            for half in range(1, HALVES):
+                mix.append(
+                    spread_to(rows_all, pl.ds(half * half_rows, half_rows), m_send, m_recv, half)
+                )
+        complete([h_stage])
+        if j == 0:
+            loads[5].wait()
+        part = jnp.dot(hidden[0, rows, :], wd_v[0:ff, :], preferred_element_type=jnp.float32)
+        for s in range(1, tp):
+            part = part + jnp.dot(
+                hidden[s, rows, :],
+                wd_v[s * ff : (s + 1) * ff, :],
+                preferred_element_type=jnp.float32,
+            )
+        results[rows, :] = part.astype(jnp.bfloat16)
+        for k in reversed(range(chunk_of(j), chunk_of(j) + per_chunk)):
+            if k > 0:
+                back[k] = pltpu.make_async_remote_copy(
+                    src_ref=results.at[block(k)],
+                    dst_ref=returned.at[block(k)],
+                    send_sem=ret_send.at[k],
+                    recv_sem=ret_recv.at[k],
+                    device_id=(e ^ k, t),
+                    device_id_type=MESH,
+                )
+                back[k].start()
+            else:
+                returned[0:pitch, :] = results[0:pitch, :]
+
+    for half in range(1, HALVES):
+        mixer(half)
+
+    for j in reversed(range(CHUNKS)):
+        for k in range(max(1, chunk_of(j)), chunk_of(j) + per_chunk):
+            back[k].wait_recv()
+        span = slice(chunk_of(j) * pitch, chunk_of(j) * pitch + chunk_rows)
+        term = jnp.dot(
+            picks[0, :, span], returned[span, :], preferred_element_type=jnp.float32
+        ) + jnp.dot(picks[1, :, span], returned[span, :], preferred_element_type=jnp.float32)
+        if j == CHUNKS - 1:
+            total[...] = term
+        else:
+            total[...] += term
+    out_ref[...] = total[...].astype(jnp.bfloat16)
+
+    for k in range(1, n):
+        xz[k].wait_send()
+        back[k].wait_send()
+    for copy in sent:
+        copy.wait_send()
+
+
+def fused_device(
+    conv_gate,
+    conv_in_gate,
+    conv_value,
+    conv_taps,
+    mix_out_weight,
+    expert_input,
+    expert_gain,
+    routes,
+    group_prob,
+    pair_logits,
+    expert_gate,
+    expert_up,
+    expert_down,
+):
+    n, tp = lax.axis_size("ep"), lax.axis_size("tp")
+    tok_b, columns = expert_input.shape
+    tok_a, channels = conv_value.shape
+    width, ff = expert_gate.shape[1:]
+    cap = 3 * tok_b * routes.shape[1] // (2 * n)
+    pitch = -(-cap // 16) * 16
+    cap = -(-cap // 8) * 8
+    slots = n * pitch
+    lane = jnp.arange(slots, dtype=jnp.int32)
+    lanes = jnp.stack([lane // pitch, lane % pitch])
+    chunk_rows = slots // CHUNKS
+    tail = 16
+    any_spec = pl.BlockSpec(memory_space=pl.ANY)
+    vmem = pl.BlockSpec(memory_space=pltpu.VMEM)
+    dma = pltpu.SemaphoreType.DMA
+    bf16, f32 = jnp.bfloat16, jnp.float32
+    return pl.pallas_call(
+        functools.partial(fused_kernel, n, cap, pitch),
+        out_shape=(
+            jax.ShapeDtypeStruct((tok_a, mix_out_weight.shape[1]), bf16),
+            jax.ShapeDtypeStruct((tok_b, columns), bf16),
+        ),
+        in_specs=[
+            any_spec, any_spec, any_spec, vmem, any_spec, vmem, vmem, vmem, vmem, vmem, vmem,
+            any_spec, any_spec, any_spec,
+        ],
+        out_specs=(vmem, vmem),
+        scratch_shapes=[
+            pltpu.VMEM((tok_a, channels), bf16),
+            pltpu.VMEM((tok_a, channels), bf16),
+            pltpu.VMEM((tok_a, channels), bf16),
+            pltpu.VMEM(mix_out_weight.shape, bf16),
+            pltpu.VMEM((width, ff), bf16),
+            pltpu.VMEM((width, ff), bf16),
+            pltpu.VMEM(expert_down.shape[1:], bf16),
+            pltpu.VMEM((2, tail, channels), bf16),
+            pltpu.VMEM((8 + tok_a, channels), f32),
+            pltpu.VMEM((tp, tok_a, channels), bf16),
+            pltpu.VMEM((2, tok_b, slots), bf16),
+            pltpu.VMEM((slots, columns), bf16),
+            pltpu.VMEM((tp, slots, columns), bf16),
+            pltpu.VMEM((chunk_rows, width), bf16),
+            pltpu.VMEM((tp, slots, ff), bf16),
+            pltpu.VMEM((slots, columns), bf16),
+            pltpu.VMEM((slots, columns), bf16),
+            pltpu.VMEM((tok_b, columns), f32),
+            dma((7,)),
+            dma((2,)),
+            dma((2,)),
+            dma((n,)),
+            dma((n,)),
+            dma((3, n)),
+            dma((3, n)),
+            dma((3, CHUNKS)),
+            dma((3, CHUNKS)),
+            dma((3, HALVES)),
+            dma((3, HALVES)),
+            dma((n,)),
+            dma((n,)),
+        ],
+        compiler_params=pltpu.CompilerParams(
+            collective_id=0, has_side_effects=True, vmem_limit_bytes=60 * 1024 * 1024
+        ),
+    )(
+        conv_gate,
+        conv_in_gate,
+        conv_value,
+        conv_taps,
+        mix_out_weight,
+        expert_input,
+        expert_gain.reshape(1, width),
+        routes,
+        group_prob.reshape(tok_b, 1),
+        pair_logits,
+        lanes,
+        expert_gate,
+        expert_up,
+        expert_down,
+    )
+
+
 def solution(mesh):
+    partners = mesh.shape["ep"]
+    fused = mesh.shape["tp"] == 2 * CORES and partners & (partners - 1) == 0
+    body = fused_device if fused else per_device
     in_specs = (
         P("ep", "tp"),
         P("ep", "tp"),
@@ -128,5 +565,5 @@
     )
     out_specs = (P("ep", "tp"), P("ep", "tp"))
     return jax.shard_map(
-        per_device, mesh=mesh, in_specs=in_specs, out_specs=out_specs, check_vma=False
-    )
+        body, mesh=mesh, in_specs=in_specs, out_specs=out_specs, check_vma=False
+    )

time: 171 us -> 103 us (0.60)
  Pallas kernels: 0 us -> 92.4 us
  waiting for transfers between devices: 70.3 us -> 0 us
  blocking collectives: 36.6 us -> 0 us
  matrix products: 19.9 us -> 0 us
  between operations: 14 us -> 0.65 us
  starting transfers between devices: 8.44 us -> 0 us
  other arithmetic: 7.81 us -> 0.61 us
  local copies, waits for them, and re-layouts: 12.3 us -> 8.27 us
    pallas_call x0 -> x1, Pallas kernels: none -> 92.4 us  [fused_device(): pl.pallas_call(functools.partial(fused_kernel, n, cap, pitch), out_shape=...]
    all_gather x3 -> x0, waiting for transfers between devices: 63.6 us -> none  [the longest x1 33.8 us: per_device(): shard_piece = lax.all_gather(arrived, 'tp', axis=1, tiled=True)]
    all_to_all x1 -> x0, blocking collectives: 30.2 us -> none  [per_device(): lax.all_to_all(buffer.reshape(expert_count, capacity, columns), 'ep', spl...]
    dot_general x4 -> x0, matrix products: 19.9 us -> none  [the longest x1 6.12 us: per_device(): jnp.dot(lax.all_gather(mixer_rows, 'tp', axis=1, tiled=True), mix_out_wei...]
    psum x1 -> x0, blocking collectives: 6.4 us -> none  [per_device(): squares = lax.psum(jnp.sum(features * features, axis=1), 'tp')]
    unnamed x17 -> x4, local copies, waits for them, and re-layouts: 0.86 us -> 6.84 us
    all_to_all x1 -> x0, waiting for transfers between devices: 5.89 us -> none  [per_device(): lax.all_to_all(results.reshape(expert_count, capacity, down_block.shape[1...]
    all_to_all x1 -> x0, starting transfers between devices: 5.23 us -> none  [per_device(): lax.all_to_all(results.reshape(expert_count, capacity, down_block.shape[1...]
  transfers between devices with their start and end apart: 5 -> 0, of which waited for: 5 -> 0; matrix products, arithmetic and copies ran while one was open for 8% -> 0% of each run, Pallas kernels for 0% -> 0%
where the time goes in v1:
time: 103 us; the launch traced here: 102 us
  Pallas kernels  92.4 us (90%)
  local copies, waits for them, and re-layouts  8.27 us (8%)
    pallas_call x1, Pallas kernels, fused_device(): pl.pallas_call(functools.partial(fused_kernel, n, cap, pitch), out_shape=...  92.4 us
    unnamed x4, local copies, waits for them, and re-layouts  6.84 us

profile of v1, /device:TPU:1, one launch (start us, length us, event | category | flops | bytes accessed | tf_op | source)
XLA Modules:
  0.0 102.0 jit_solution(3556023548942958704)
XLA Ops:
  0.6 0.6 pad_add_fusion.lanes_ref
  1.2 1.4 %copy.17.routes_ref = s32[160,2]{1,0:T(8,128)} copy(s32[160,2]{0,1:T(2,128)} %param.20) | data formatting | bytes 2560 | tf_op args[7]
  2.7 1.4 %copy.18.prob_ref = f32[160,1]{1,0:T(8,128)} copy(f32[160,1]{0,1:T(1,128)} %bitcast.3) | data formatting | bytes 1280 | tf_op jit(solution)/shard_map/reshape | solution.py:538
  4.1 1.4 %copy.19.logits_ref = f32[160,2]{1,0:T(8,128)} copy(f32[160,2]{0,1:T(2,128)} %param.22) | data formatting | bytes 2560 | tf_op args[9]
  5.5 92.4 %shard_map.140 = (bf16[512,1024]{1,0:T(8,128)(2,1)}, bf16[160,1024]{1,0:T(8,128)(2,1)}) custom-call(bf16[512,512]{1,0:T(8,128)(2,1)} %gate_h.1, bf16[512,512]{1,0:T(8,128)(2,1)} %ingate_h.1, bf16[512,512]{1,0:T(8,128)(2,1)} %value_h.1, f32[3,512]{1,0:T(4,128)} %taps_ref.1, bf16[2048,1024]{1,0:T(8,128)(2,1)} %wmix_h.1, bf16[160,1024]{1,0:T(8,128)(2,1)} %x_ref.1, ...), custom_call_target="tpu_custom_call" | custom-call | tf_op jit(solution)/shard_map/pallas_call | solution.py:482
  98.0 2.3 %copy.22 = bf16[512,1024]{1,0:T(8,128)(2,1)} copy(bf16[512,1024]{1,0:T(8,128)(2,1)} %get-tuple-element.6) | data formatting | bytes 2097152
  100.2 1.7 %copy.23 = bf16[160,1024]{1,0:T(8,128)(2,1)} copy(bf16[160,1024]{1,0:T(8,128)(2,1)} %get-tuple-element.7) | data formatting | bytes 655360
  (1 shorter events, 0.0 us)

commit v2 on v1

--- a/solution.py
+++ b/solution.py
@@ -117,6 +117,7 @@
 CHUNKS = 2
 CORES = 2
 HALVES = 2
+EARLY = 1
 MESH = pl.DeviceIdType.MESH
 
 
@@ -134,7 +135,6 @@
     routes_ref,
     prob_ref,
     logits_ref,
-    lanes_ref,
     wg_h,
     wu_h,
     wd_h,
@@ -217,25 +217,33 @@
     def block(k):
         return pl.ds(k * pitch, cap)
 
-    expert_of = lanes_ref[0:1, :] ^ e
-    place_of = lanes_ref[1:2, :]
-    first = (routes_ref[:, 0:1] == expert_of).astype(jnp.float32)
-    second = (routes_ref[:, 1:2] == expert_of).astype(jnp.float32)
+    lane = lax.broadcasted_iota(jnp.int32, (1, n * pitch), 1)
+    partner = jnp.zeros_like(lane)
+    for k in range(1, n):
+        partner = partner + (lane >= k * pitch).astype(jnp.int32)
+    expert_of = (partner ^ e).astype(jnp.float32)
+    place_of = lane - partner * pitch
+    row_at = lax.broadcasted_iota(jnp.int32, (tok_b, tok_b), 0)
+    lane_at = lax.broadcasted_iota(jnp.int32, (tok_b, tok_b), 1)
+
+    def column(row):
+        return jnp.sum(jnp.where(row_at == lane_at, row, 0.0), axis=1, keepdims=True)
+
+    routes_f = routes_ref[...].astype(jnp.float32)
+    first = (column(routes_f[0:1, :]) == expert_of).astype(jnp.float32)
+    second = (column(routes_f[1:2, :]) == expert_of).astype(jnp.float32)
     named = first + second
-    earlier = (
-        lax.broadcasted_iota(jnp.int32, (tok_b, tok_b), 1)
-        < lax.broadcasted_iota(jnp.int32, (tok_b, tok_b), 0)
-    ).astype(jnp.float32)
+    earlier = (lane_at < row_at).astype(jnp.float32)
     within = jnp.dot(
         earlier.astype(jnp.bfloat16),
         named.astype(jnp.bfloat16),
         preferred_element_type=jnp.float32,
     )
     here = (within == place_of.astype(jnp.float32)).astype(jnp.float32)
-    spread = logits_ref[:, 0:1] - logits_ref[:, 1:2]
+    spread = logits_ref[0:1, :] - logits_ref[1:2, :]
     prob = prob_ref[...]
-    w_first = prob * jax.nn.sigmoid(spread)
-    w_second = prob * jax.nn.sigmoid(-spread)
+    w_first = column(prob * jax.nn.sigmoid(spread))
+    w_second = column(prob * jax.nn.sigmoid(-spread))
     pick = named * here
     weighted = (first * w_first + second * w_second) * here
     high = weighted.astype(jnp.bfloat16)
@@ -250,52 +258,6 @@
     arrived[t, 0:pitch, :] = outgoing[0:pitch, :]
 
     pl.semaphore_wait(barrier, n + 1)
-
-    xz = [None]
-    for k in range(1, n):
-        xz.append(
-            pltpu.make_async_remote_copy(
-                src_ref=outgoing.at[block(k)],
-                dst_ref=arrived.at[t, block(k)],
-                send_sem=xz_send.at[k],
-                recv_sem=xz_recv.at[k],
-                device_id=(e ^ k, t),
-                device_id_type=MESH,
-            )
-        )
-    for k in reversed(range(1, n)):
-        xz[k].start()
-
-    sent = []
-
-    def spread_to(ref, sel, sends, recvs, at):
-        def copy(s, way, target):
-            return pltpu.make_async_remote_copy(
-                src_ref=ref.at[s, sel],
-                dst_ref=ref.at[s, sel],
-                send_sem=sends.at[way, at],
-                recv_sem=recvs.at[way, at],
-                device_id=(e, target),
-                device_id_type=MESH,
-            )
-
-        far, near = copy(t, 0, t_far), copy(t, 1, t_core)
-        far.start()
-        near.start()
-        sent.append(far)
-        sent.append(near)
-
-        def relay():
-            copy(t_far, 0, t_far).wait_recv()
-            passed = copy(t_far, 2, t_core)
-            passed.start()
-            sent.append(passed)
-
-        def finish():
-            copy(t_core, 1, t_core).wait_recv()
-            copy(t_far_core, 2, t_core).wait_recv()
-
-        return relay, finish
 
     loads[0].wait()
     loads[1].wait()
@@ -313,6 +275,53 @@
     ]
     for copy in tails:
         copy.start()
+
+    xz = [None]
+    for k in range(1, n):
+        xz.append(
+            pltpu.make_async_remote_copy(
+                src_ref=outgoing.at[block(k)],
+                dst_ref=arrived.at[t, block(k)],
+                send_sem=xz_send.at[k],
+                recv_sem=xz_recv.at[k],
+                device_id=(e ^ k, t),
+                device_id_type=MESH,
+            )
+        )
+    for k in reversed(range(1, n)):
+        xz[k].start()
+
+    sent = []
+
+    def spread_to(ref, sel, sends, recvs, at):
+        def copy(s, way, target):
+            return pltpu.make_async_remote_copy(
+                src_ref=ref.at[s, sel],
+                dst_ref=ref.at[s, sel],
+                send_sem=sends.at[way, at],
+                recv_sem=recvs.at[way, at],
+                device_id=(e, target),
+                device_id_type=MESH,
+            )
+
+        far, near = copy(t, 0, t_far), copy(t, 1, t_core)
+        far.start()
+        near.start()
+        sent.append(far)
+        sent.append(near)
+
+        def relay():
+            copy(t_far, 0, t_far).wait_recv()
+            passed = copy(t_far, 2, t_core)
+            passed.start()
+            sent.append(passed)
+
+        def finish():
+            copy(t_core, 1, t_core).wait_recv()
+            copy(t_far_core, 2, t_core).wait_recv()
+
+        return relay, finish
+
     top = 8
     padded[top:, :] = ingate_v[...].astype(jnp.float32) * value_v[...].astype(jnp.float32)
     for copy in tails:
@@ -335,18 +344,23 @@
             gate_v[pl.ds(base, half_rows), :].astype(jnp.float32) * convolved
         ).astype(jnp.bfloat16)
     mix = []
-    mix.append(spread_to(rows_all, pl.ds(0, half_rows), m_send, m_recv, 0))
+
+    def spread_rows(half):
+        mix.append(spread_to(rows_all, pl.ds(half * half_rows, half_rows), m_send, m_recv, half))
+
+    for half in range(EARLY):
+        spread_rows(half)
 
     def chunk_of(j):
         return (CHUNKS - 1 - j) * per_chunk
 
-    def forward(j):
-        stages = []
-        for k in reversed(range(chunk_of(j), chunk_of(j) + per_chunk)):
-            if k > 0:
-                xz[k].wait_recv()
-            stages.append(spread_to(arrived, block(k), xt_send, xt_recv, k))
-        return stages
+    def forward(k):
+        if k > 0:
+            xz[k].wait_recv()
+        return spread_to(arrived, block(k), xt_send, xt_recv, k)
+
+    def partners(j):
+        return list(reversed(range(chunk_of(j), chunk_of(j) + per_chunk)))
 
     def complete(stages):
         for relay, _ in stages:
@@ -369,7 +383,12 @@
         mixed_ref[rows, :] = part.astype(jnp.bfloat16)
 
     back = {}
-    stages = forward(0)
+    order = partners(0)
+    stages = [forward(k) for k in order[: per_chunk // 2]]
+    loads[6].wait()
+    for half in range(EARLY):
+        mixer(half)
+    stages += [forward(k) for k in order[per_chunk // 2 :]]
     for j in range(CHUNKS):
         rows = pl.ds(chunk_of(j) * pitch, chunk_rows)
         complete(stages)
@@ -390,16 +409,11 @@
         up_sum = jnp.dot(normed[...], wu_v[...], preferred_element_type=jnp.float32)
         hidden[t, rows, :] = (gate_sum / (1.0 + jnp.exp(-gate_sum)) * up_sum).astype(jnp.bfloat16)
         h_stage = spread_to(hidden, rows, h_send, h_recv, j)
-        if j == 0:
-            loads[6].wait()
-            mixer(0)
         if j + 1 < CHUNKS:
-            stages = forward(j + 1)
+            stages = [forward(k) for k in partners(j + 1)]
         else:
-            for half in range(1, HALVES):
-                mix.append(
-                    spread_to(rows_all, pl.ds(half * half_rows, half_rows), m_send, m_recv, half)
-                )
+            for half in range(EARLY, HALVES):
+                spread_rows(half)
         complete([h_stage])
         if j == 0:
             loads[5].wait()
@@ -425,7 +439,7 @@
             else:
                 returned[0:pitch, :] = results[0:pitch, :]
 
-    for half in range(1, HALVES):
+    for half in range(EARLY, HALVES):
         mixer(half)
 
     for j in reversed(range(CHUNKS)):
@@ -446,6 +460,11 @@
         back[k].wait_send()
     for copy in sent:
         copy.wait_send()
+
+
+def hand_over(mixed_in, out_in, mixed_ref, out_ref):
+    mixed_ref[...] = mixed_in[...]
+    out_ref[...] = out_in[...]
 
 
 def fused_device(
@@ -471,22 +490,20 @@
     pitch = -(-cap // 16) * 16
     cap = -(-cap // 8) * 8
     slots = n * pitch
-    lane = jnp.arange(slots, dtype=jnp.int32)
-    lanes = jnp.stack([lane // pitch, lane % pitch])
     chunk_rows = slots // CHUNKS
     tail = 16
     any_spec = pl.BlockSpec(memory_space=pl.ANY)
     vmem = pl.BlockSpec(memory_space=pltpu.VMEM)
     dma = pltpu.SemaphoreType.DMA
     bf16, f32 = jnp.bfloat16, jnp.float32
-    return pl.pallas_call(
+    outputs = pl.pallas_call(
         functools.partial(fused_kernel, n, cap, pitch),
         out_shape=(
             jax.ShapeDtypeStruct((tok_a, mix_out_weight.shape[1]), bf16),
             jax.ShapeDtypeStruct((tok_b, columns), bf16),
         ),
         in_specs=[
-            any_spec, any_spec, any_spec, vmem, any_spec, vmem, vmem, vmem, vmem, vmem, vmem,
+            any_spec, any_spec, any_spec, vmem, any_spec, vmem, vmem, vmem, vmem, vmem,
             any_spec, any_spec, any_spec,
         ],
         out_specs=(vmem, vmem),
@@ -534,14 +551,19 @@
         mix_out_weight,
         expert_input,
         expert_gain.reshape(1, width),
-        routes,
-        group_prob.reshape(tok_b, 1),
-        pair_logits,
-        lanes,
+        routes.T,
+        group_prob.reshape(1, tok_b),
+        pair_logits.T,
         expert_gate,
         expert_up,
         expert_down,
     )
+    return pl.pallas_call(
+        hand_over,
+        out_shape=tuple(jax.ShapeDtypeStruct(o.shape, o.dtype) for o in outputs),
+        in_specs=[vmem, vmem],
+        out_specs=(vmem, vmem),
+    )(*outputs)
 
 
 def solution(mesh):

time: 103 us -> 85.9 us (0.83)
  local copies, waits for them, and re-layouts: 8.27 us -> 0 us
  Pallas kernels: 92.4 us -> 85.1 us
    pallas_call x1, Pallas kernels: 92.4 us -> 82.7 us  [fused_device(): pl.pallas_call(functools.partial(fused_kernel, n, cap, pitch), out_shape=...]
    unnamed x4 -> x0, local copies, waits for them, and re-layouts: 6.84 us -> none
    pallas_call x0 -> x1, Pallas kernels: none -> 2.43 us  [fused_device(): pl.pallas_call(hand_over, out_shape=tuple((jax.ShapeDtypeStruct(o.shape,...]
    reshape x1 -> x0, local copies, waits for them, and re-layouts: 1.43 us -> none  [fused_device(): group_prob.reshape(tok_b, 1)]
where the time goes in v2:
time: 85.9 us; the launch traced here: 85.7 us
  Pallas kernels  85.1 us (99%)
    pallas_call x1, Pallas kernels, fused_device(): pl.pallas_call(functools.partial(fused_kernel, n, cap, pitch), out_shape=...  82.7 us
    pallas_call x1, Pallas kernels, fused_device(): pl.pallas_call(hand_over, out_shape=tuple((jax.ShapeDtypeStruct(o.shape,...  2.43 us

profile of v2, /device:TPU:1, one launch (start us, length us, event | category | flops | bytes accessed | tf_op | source)
XLA Modules:
  0.0 85.7 jit_solution(5942701071534056115)
XLA Ops:
  0.6 82.7 %shard_map.140 = (bf16[512,1024]{1,0:T(8,128)(2,1)}, bf16[160,1024]{1,0:T(8,128)(2,1)}) custom-call(bf16[512,512]{1,0:T(8,128)(2,1)} %gate_h.1, bf16[512,512]{1,0:T(8,128)(2,1)} %ingate_h.1, bf16[512,512]{1,0:T(8,128)(2,1)} %value_h.1, f32[3,512]{1,0:T(4,128)} %taps_ref.1, bf16[2048,1024]{1,0:T(8,128)(2,1)} %wmix_h.1, bf16[160,1024]{1,0:T(8,128)(2,1)} %x_ref.1, ...), custom_call_target="tpu_custom_call" | custom-call | tf_op jit(solution)/shard_map/pallas_call | solution.py:499
  83.3 2.4 %shard_map.141 = (bf16[512,1024]{1,0:T(8,128)(2,1)}, bf16[160,1024]{1,0:T(8,128)(2,1)}) custom-call(bf16[512,1024]{1,0:T(8,128)(2,1)} %get-tuple-element.4.mixed_in, bf16[160,1024]{1,0:T(8,128)(2,1)} %get-tuple-element.5.out_in), custom_call_target="tpu_custom_call" | custom-call | tf_op jit(solution)/shard_map/pallas_call | solution.py:561
